TPU v7x, 32 devices: a whole 2x2x4 slice. The times are simulated.
32 devices in a mesh: sp: 4 (over z), tp: 2 (over y), dp: 4 (over x, core).
Axes of the slice: x: 2, y: 2, z: 4, core: 2. Of those that a mesh axis runs over, the one named last changes fastest.
Arguments:
- latents: bfloat16 [4, 2048, 3072], P('dp', ('sp', 'tp')), may hold values from -5 to 5
- condition: bfloat16 [4, 3072], P('dp', ('sp', 'tp')), may hold values from -6 to 6
- context: bfloat16 [4, 384, 3072], P('dp', ('sp', 'tp')), may hold values from -6 to 6
- context_cond: bfloat16 [3072], P(('sp', 'tp')), may hold values from -6 to 6
- shift_weight: bfloat16 [3072, 3072], P(('sp', 'tp')), may hold values from -0.109375 to 0.109375
- scale_weight: bfloat16 [3072, 3072], P(('sp', 'tp')), may hold values from -0.109375 to 0.109375
- out_gate_weight: bfloat16 [3072, 3072], P(('sp', 'tp')), may hold values from -0.109375 to 0.109375
- pre_gain: float32 [3072], replicated, may hold values from 0.1 to 1.9
- post_gain: float32 [3072], replicated, may hold values from 0.1 to 1.9
- query_weight: bfloat16 [3072, 1024], P(None, 'tp'), may hold values from -0.108253175 to 0.108253175
- key_weight: bfloat16 [3072, 256], replicated, may hold values from -0.108253175 to 0.108253175
- value_weight: bfloat16 [3072, 256], replicated, may hold values from -0.109375 to 0.109375
- head_gate_weight: bfloat16 [3072, 1024], P(None, 'tp'), may hold values from -0.109375 to 0.109375
- lambdas: float32 [8], P('tp'), may hold values from 0.3 to 0.8
- head_gain: float32 [128], replicated, may hold values from 0.1 to 1.9
- out_weight: bfloat16 [1024, 3072], P(None, 'tp'), may hold values from -0.1875 to 0.1875
Outputs:
- mixed_out: bfloat16 [4, 2048, 3072], P('dp', ('sp', 'tp'))
All inputs are finite; a program needn't handle non-finite values.
Results may differ from a plain program's by a relative error of at most 0.0128.
The roundings to bfloat16 on the way count: a program that leaves them out, or rounds other values in their place, can miss the bound.
Values may be sent and summed in bfloat16 or wider, within the bound.
A program may use at most 64 MiB of HBM per device.

v0:
```python
import functools
import math

import jax
import jax.numpy as jnp
from jax import lax
from jax.experimental import pallas as pl
from jax.experimental.pallas import tpu as pltpu
from jax.sharding import PartitionSpec as P

HEADS = 8
KVH = 2
HQK = 64
HV = 128
NORM_EPSILON = 1e-06
MESH = pl.DeviceIdType.MESH
SUBLANES = 16
LANES = 128


def norm_rows(values):
    return values * lax.rsqrt(jnp.mean(values * values, axis=-1, keepdims=True) + NORM_EPSILON)


def each(count, body):
    if count <= 8:
        for index in range(count):
            body(index)
    else:
        pl.loop(0, count)(body)


def only(always, condition, body):
    if always:
        body()
    else:
        pl.when(condition)(body)


def flip(index, bit):
    return index + bit - 2 * bit * lax.rem(index // bit, 2)


def lanes(start, size):
    return pl.ds(pl.multiple_of(start, LANES), size)


def rows_at(start, size):
    return pl.ds(pl.multiple_of(start, math.gcd(size, SUBLANES)), size)


class Plan:
    def __init__(self, sp, tp, dp, rows, context, model, weight_shape, query_columns):
        self.sp, self.tp, self.dp = sp, tp, dp
        self.group = sp * tp
        self.rows, self.context, self.model = rows, context, model
        self.columns = query_columns
        self.local_heads = query_columns // (2 * HQK)
        self.per_group = (HEADS // KVH) // self.local_heads
        self.used = rows + context
        self.padded = -(-self.used // SUBLANES) * SUBLANES
        self.owners = math.gcd(model // LANES, self.group)
        self.slice = model // self.owners
        self.depth, self.out_columns = weight_shape
        self.quarter = self.depth // dp
        self.pair = math.gcd(math.gcd(sp, 2), self.quarter // SUBLANES)
        self.share = self.quarter // self.pair
        self.parts = math.gcd(4, self.share // SUBLANES)
        self.unit = max(SUBLANES, rows // 4 // SUBLANES * SUBLANES)
        self.units = rows // self.unit
        self.stack = self.local_heads * 2 * self.unit
        self.half = self.stack // 2
        self.halves = 2 if self.unit % (2 * SUBLANES) == 0 else 1
        self.near = (tp + sp - 1) * self.padded
        self.far = (tp - 1) * (sp - 1) * self.padded
        self.groups = [[0]] + [[chunk] for chunk in range(1, self.units)]
        if self.units > 2:
            self.groups = [[0, 1]] + [[chunk] for chunk in range(2, self.units)]


def modulate_rows(source, target, start, count, target_start, gain_scale, shift):
    block = math.gcd(count, 32)

    def step(index):
        offset = pl.multiple_of(index * block, block)
        values = norm_rows(source[pl.ds(start + offset, block), :].astype(jnp.float32))
        result = values * gain_scale + shift
        target[pl.ds(target_start + offset, block), :] = result.astype(jnp.bfloat16)

    pl.loop(0, count // block)(step)


def mega_kernel(
    plan,
    lambda_ref, cond_ref, context_cond_ref, gain_ref, post_gain_ref, head_gain_ref,
    latents, context, shift_weight, scale_weight, gate_weight,
    query_weight, key_weight, value_weight, head_gate_weight, out_weight,
    out_ref,
    wcond, own_rows, own_context, own_in, kv_weight, q_weight, g_weight, own_out_weight,
    other_out_weight, other_rows, other_in, kv_made, kv, parts, held, sums, normed,
    queries, gates, scores_a, scores_b, weighted, normalizer, largest, branch, back, projected,
    load_sem, sum_send, sum_recv, all_send, all_recv,
    row_send, row_recv, kvy_send, kvy_recv, kvz_send, kvz_recv,
    wy_send, wy_recv, wz_send, wz_recv, wx_send, wx_recv, wd_send, wd_recv,
    back_send, back_recv,
):
    sp, tp, dp, group = plan.sp, plan.tp, plan.dp, plan.group
    s, t, d = lax.axis_index("sp"), lax.axis_index("tp"), lax.axis_index("dp")
    me = s * tp + t
    rows, context_rows, unit, units = plan.rows, plan.context, plan.unit, plan.units
    heads, columns, size = plan.local_heads, plan.columns, plan.padded
    f32, bf16 = jnp.float32, jnp.bfloat16

    def load(index, source, target):
        copy = pltpu.make_async_copy(source, target, load_sem.at[index])
        copy.start()
        return copy

    cond_loads = [
        load(i, w, wcond.at[i]) for i, w in enumerate((shift_weight, scale_weight, gate_weight))
    ]
    row_load = load(3, latents, own_rows)
    context_load = load(4, context, own_context)
    def member(offset):
        other = lax.rem(me + offset, group)
        return {"sp": other // tp, "tp": lax.rem(other, tp)}

    def remote(source, target, send, recv, device):
        return pltpu.make_async_remote_copy(
            src_ref=source, dst_ref=target, send_sem=send, recv_sem=recv,
            device_id=device, device_id_type=MESH,
        )

    bits = []
    bit = dp // 2
    while bit:
        bits.append(bit)
        bit //= 2

    barrier = pltpu.get_barrier_semaphore()

    def greet(index):
        pl.semaphore_signal(
            barrier, inc=1, device_id=member(index + 1), device_id_type=MESH
        )

    each(group - 1, greet)
    for bit in bits:
        pl.semaphore_signal(
            barrier, inc=1, device_id={"dp": flip(d, bit)}, device_id_type=MESH
        )

    base = s - lax.rem(s, plan.pair)
    ring = lax.rem(s, plan.pair)
    piece = plan.share // plan.parts

    def over_tp(step):
        return {"tp": lax.rem(t + step, tp)}

    def weight_y(step, part):
        at = rows_at((d * plan.pair + ring) * plan.share + part * piece, piece)
        return remote(
            out_weight.at[at, :], other_out_weight.at[step - 1, at, :],
            wy_send.at[step - 1, part], wy_recv.at[step - 1, part], over_tp(step),
        )

    def weight_z(step, turn, part):
        at = rows_at((d * plan.pair + ring) * plan.share + part * piece, piece)
        return remote(
            other_out_weight.at[step - 1, at, :], other_out_weight.at[step - 1, at, :],
            wz_send.at[step - 1, turn - 1, part], wz_recv.at[step - 1, turn - 1, part],
            {"sp": base + lax.rem(ring + turn, plan.pair)},
        )

    def weight_x(step, turn, part):
        source = lax.rem(ring + turn, plan.pair)
        at = rows_at((d * plan.pair + source) * plan.share + part * piece, piece)
        return remote(
            other_out_weight.at[step - 1, at, :], other_out_weight.at[step - 1, at, :],
            wx_send.at[step - 1, turn, part], wx_recv.at[step - 1, turn, part],
            {"dp": flip(d, bits[0])},
        )

    def weight_d(step, level, index):
        turns = [0]
        for earlier in bits[:level]:
            turns += [turn ^ earlier for turn in turns]
        source = d
        for other in bits:
            if turns[index] & other:
                source = flip(source, other)
        at = rows_at(source * plan.quarter, plan.quarter)
        slot = (2**level - 1) + index
        return remote(
            other_out_weight.at[step - 1, at, :], other_out_weight.at[step - 1, at, :],
            wd_send.at[step - 1, slot], wd_recv.at[step - 1, slot],
            {"dp": flip(d, bits[level])},
        )

    def level_copies(step, level):
        if level == 0:
            return [
                weight_x(step, turn, part)
                for turn in range(plan.pair) for part in range(plan.parts)
            ]
        return [weight_d(step, level, index) for index in range(2**level)]

    def row_copy(step, chunk):
        at = pl.ds(chunk * unit, unit)
        return remote(
            latents.at[at, :], other_rows.at[step - 1, at, :],
            row_send.at[step - 1, chunk], row_recv.at[step - 1, chunk], over_tp(step),
        )

    def over_tp_steps(body):
        for step in range(1, tp):
            body(step)

    with jax.named_scope("enter"):
        pl.semaphore_wait(barrier, group - 1 + len(bits))

    def weight_start(part):
        if part < plan.parts:
            over_tp_steps(lambda step: weight_y(step, part).start())

    def weight_forward(part):
        if part < plan.parts:
            for step in range(1, tp):
                weight_y(step, part).wait_recv()
                if bits:
                    weight_x(step, 0, part).start()
                for turn in range(1, plan.pair):
                    weight_z(step, turn, part).start()

    weight_start(0)

    with jax.named_scope("conditions"):
        conditions = []
        for ref in (cond_ref, context_cond_ref):
            value = ref[...].astype(f32)
            conditions.append(value / (1.0 + jnp.exp(-value)))
        depth = cond_ref.shape[1]
        index = lax.broadcasted_iota(jnp.int32, (8, depth), 0)
        first = jnp.broadcast_to(conditions[0], (8, depth))
        second = jnp.broadcast_to(conditions[1], (8, depth))
        lefts = []
        for number in range(3):
            left = jnp.where(index == 2 * number, first, 0.0)
            if number < 2:
                left = jnp.where(index == 2 * number + 1, second, left)
            lefts.append(left.astype(bf16))
        width = plan.slice
        for copy in cond_loads:
            copy.wait()
        kv_loads = []
        for head in range(KVH):
            for part, weight in enumerate((key_weight, value_weight)):
                kv_loads.append(
                    load(
                        5 + 2 * head + part,
                        weight.at[:, pl.ds(head * LANES, LANES)],
                        kv_weight.at[:, pl.ds((2 * head + part) * LANES, LANES)],
                    )
                )
        late_loads = [
            load(5 + 2 * KVH, query_weight, q_weight),
            load(6 + 2 * KVH, head_gate_weight, g_weight),
        ]
        tail_load = load(7 + 2 * KVH, out_weight, own_out_weight)

        def partial_sums(column):
            at = lanes(column * width, width)
            total = None
            for number in range(3):
                part = jnp.dot(lefts[number], wcond[number, :, at], preferred_element_type=f32)
                total = part if total is None else total + part
            parts[:, at] = total

        each(plan.owners, partial_sums)

    every = plan.owners == group

    def scatter(index):
        owner = lax.rem(me + index + 1, group)
        return remote(
            parts.at[:, lanes(lax.rem(owner, plan.owners) * width, width)],
            held.at[index], sum_send.at[index], sum_recv.at[index], member(index + 1),
        ), owner < plan.owners

    def scatter_start(index):
        copy, valid = scatter(index)
        only(every, valid, copy.start)

    each(group - 1, scatter_start)

    weight_start(1)
    row_load.wait()
    block = math.gcd(rows, 32)

    def normalize(index):
        at = pl.ds(pl.multiple_of(index * block, block), block)
        normed[at, :] = norm_rows(own_rows[at, :].astype(f32))

    with jax.named_scope("normalize"):
        pl.loop(0, rows // block)(normalize)
        context_load.wait()
        normed[rows : rows + context_rows, :] = norm_rows(own_context[...].astype(f32))

    own_slice = lanes(lax.rem(me, plan.owners) * width, width)

    def gather(index):
        return remote(
            sums.at[:, own_slice], sums.at[:, own_slice],
            all_send.at[index], all_recv.at[index], member(index + 1),
        )

    def arrived(index):
        origin = lax.rem(me + group - index - 1, group)
        at = lanes(lax.rem(origin, plan.owners) * width, width)
        return remote(
            sums.at[:, at], sums.at[:, at],
            all_send.at[index], all_recv.at[index], member(index + 1),
        ), origin < plan.owners

    def own_sum():
        each(group - 1, lambda index: scatter(index)[0].wait_recv())
        total = parts[:, own_slice]
        if group <= 16:
            for index in range(group - 1):
                total = total + held[index]
        else:
            total = lax.fori_loop(
                0, group - 1, lambda index, value: value + held[index], total
            )
        sums[:, own_slice] = total
        each(group - 1, lambda index: gather(index).start())

    with jax.named_scope("reduce"):
        only(every, me < plan.owners, own_sum)

    weight_start(2)
    weight_start(3)
    kv[:, 2 * LANES :] = jnp.ones((kv.shape[0], LANES), bf16)

    def sum_arrival(index):
        copy, valid = arrived(index)
        only(every, valid, copy.wait_recv)

    with jax.named_scope("gather"):
        each(group - 1, sum_arrival)
    gain = gain_ref[...]
    shift, context_shift = sums[0:1, :], sums[1:2, :]
    gain_scale, context_gain_scale = gain * (1.0 + sums[2:3, :]), gain * (1.0 + sums[3:4, :])
    with jax.named_scope("modulate"):

        def modulate(index):
            at = pl.ds(pl.multiple_of(index * block, block), block)
            own_in[at, :] = (normed[at, :] * gain_scale + shift).astype(bf16)

        pl.loop(0, rows // block)(modulate)
        values = normed[rows : rows + context_rows, :] * context_gain_scale + context_shift
        if size > plan.used:
            fill = jnp.zeros((size - plan.used, plan.model), f32)
            values = jnp.concatenate([values, fill], axis=0)
        own_in[rows:, :] = values.astype(bf16)
    for copy in kv_loads:
        copy.wait()

    def make_kv(head):
        kv_made[head] = jnp.dot(
            own_in[...], kv_weight[:, lanes(head * 2 * LANES, 2 * LANES)],
            preferred_element_type=f32,
        ).astype(bf16)

    with jax.named_scope("make_kv"):
        pl.loop(0, KVH)(make_kv)

    def kv_slot(step, offset):
        slot = step if offset == 0 else tp + step * (sp - 1) + offset - 1
        return kv.at[pl.ds(slot * size, size), pl.ds(0, 2 * LANES)]

    def kv_group(column):
        return column // plan.per_group

    def kv_y(step):
        return remote(
            kv_made.at[kv_group(lax.rem(t + step, tp))], kv_slot(step, 0),
            kvy_send.at[step - 1], kvy_recv.at[step - 1], over_tp(step),
        )

    def kv_z(step, offset):
        source = kv_made.at[kv_group(t)] if step == 0 else kv_slot(step, 0)
        return remote(
            source, kv_slot(step, offset),
            kvz_send.at[step, offset - 1], kvz_recv.at[step, offset - 1],
            {"sp": lax.rem(s + offset, sp)},
        )

    over_tp_steps(lambda step: kv_y(step).start())
    own_block = load(8 + 2 * KVH, kv_made.at[kv_group(t)], kv_slot(0, 0))
    for offset in range(1, sp):
        kv_z(0, offset).start()
    for chunk in range(units):
        over_tp_steps(lambda step, chunk=chunk: row_copy(step, chunk).start())

    def project_rows(source, start, count, first_unit):
        wide = math.gcd(columns, 512)

        def make_queries(index):
            result = jnp.dot(
                source[pl.ds(start, count), :], q_weight[:, lanes(index * wide, wide)],
                preferred_element_type=f32,
            ).astype(bf16).astype(f32) * HQK ** (-0.5)
            lane = lax.broadcasted_iota(jnp.int32, (count, LANES), 1)
            for local in range(wide // LANES):
                value = result[:, local * LANES : (local + 1) * LANES]
                head = index * (wide // LANES) + local
                for number in range(2):
                    half = jnp.where((lane < HQK) == (number == 0), value, 0.0).astype(bf16)
                    for block in range(count // unit):
                        at = rows_at((head * 2 + number) * unit, unit)
                        queries[first_unit + block, at, :] = half[
                            block * unit : (block + 1) * unit
                        ]

        def make_gates(index):
            at = lanes(index * wide, wide)
            result = jnp.dot(
                source[pl.ds(start, count), :], g_weight[:, at], preferred_element_type=f32
            ).astype(bf16)
            for block in range(count // unit):
                gates[first_unit + block, :, at] = result[block * unit : (block + 1) * unit]

        pl.loop(0, columns // wide)(make_queries)
        pl.loop(0, columns // wide)(make_gates)

    for copy in late_loads:
        copy.wait()
    with jax.named_scope("own_project"):
        project_rows(own_in, 0, rows, 0)

    with jax.named_scope("kv_over_tp"):
        for step in range(1, tp):
            kv_y(step).wait_recv()
            for offset in range(1, sp):
                kv_z(step, offset).start()

    with jax.named_scope("weight_forward"):
        for part in range(plan.parts):
            weight_forward(part)

    def weight_pair_done():
        with jax.named_scope("weight_pair"):
            for step in range(1, tp):
                for turn in range(1, plan.pair):
                    for part in range(plan.parts):
                        weight_z(step, turn, part).wait_recv()
                        if bits:
                            weight_x(step, turn, part).start()

    contract = (((1,), (1,)), ((), ()))

    spans = ((0, plan.near), (plan.near, plan.far))

    def score(buffer, index, side, phase):
        begin, count = spans[phase]
        result = lax.dot_general(
            queries[index, pl.ds(side * plan.half, plan.half), :],
            kv[pl.ds(begin, count), pl.ds(0, LANES)],
            contract, preferred_element_type=f32,
        )
        if plan.used < size:
            column = lax.broadcasted_iota(jnp.int32, result.shape, 1)
            result = jnp.where(lax.rem(column, size) < plan.used, result, -jnp.inf)
        buffer[:, pl.ds(0, count)] = result

    def gather_values(buffer, index, side, phase):
        begin, count = spans[phase]
        at = pl.ds(side * plan.half, plan.half)
        scores = buffer[:, pl.ds(0, count)]
        top = jnp.max(scores, axis=-1, keepdims=True)
        if phase:
            before = largest[index, at, pl.ds(0, 1)]
            top = jnp.maximum(top, before)
        both = jnp.dot(
            jnp.exp(scores - top).astype(bf16), kv[pl.ds(begin, count), pl.ds(LANES, 2 * LANES)],
            preferred_element_type=f32,
        )
        if phase:
            keep = jnp.exp(before - top)
            weighted[index, at, :] = weighted[index, at, :] * keep + both[:, :LANES]
            normalizer[index, at, :] = normalizer[index, at, :] * keep + both[:, LANES:]
        else:
            weighted[index, at, :] = both[:, :LANES]
            normalizer[index, at, :] = both[:, LANES:]
            largest[index, at, :] = jnp.broadcast_to(top, (plan.half, LANES))

    def attend(first_unit, count, phase):
        if not spans[phase][1]:
            return
        score(scores_a, first_unit, 0, phase)

        def step(index):
            here = first_unit + index
            score(scores_b, here, 1, phase)
            gather_values(scores_a, here, 0, phase)
            score(scores_a, here + 1, 0, phase)
            gather_values(scores_b, here, 1, phase)

        if count > 1:
            pl.loop(0, count - 1)(step)
        score(scores_b, first_unit + count - 1, 1, phase)
        gather_values(scores_a, first_unit + count - 1, 0, phase)
        gather_values(scores_b, first_unit + count - 1, 1, phase)

    def finish(index, target):
        for head in range(heads):
            ratios = []
            for number in range(2):
                at = pl.ds((head * 2 + number) * unit, unit)
                ratios.append(weighted[index, at, :] / normalizer[index, at, :])
            attended = ratios[0] - lambda_ref[head] * ratios[1]
            gate = gates[index, :, pl.ds(head * LANES, LANES)].astype(f32)
            gate = gate / (1.0 + jnp.exp(-gate))
            target(head, (norm_rows(attended) * head_gain_ref[...] * gate).astype(bf16))

    def finish_own(index):
        at = rows_at(index * unit, unit)

        def store(head, value):
            branch[at, lanes(t * columns + head * LANES, LANES)] = value

        finish(index, store)

    def returned(step, chunk):
        at = pl.ds(chunk * unit, unit)
        return remote(
            back.at[step - 1, at, :], branch.at[at, lanes(t * columns, columns)],
            back_send.at[step - 1, chunk], back_recv.at[step - 1, chunk],
            over_tp(tp - step),
        )

    def returned_here(step, chunk):
        owner = lax.rem(t + step, tp)
        at = pl.ds(chunk * unit, unit)
        return remote(
            back.at[step - 1, at, :], branch.at[at, lanes(owner * columns, columns)],
            back_send.at[step - 1, chunk], back_recv.at[step - 1, chunk],
            over_tp(tp - step),
        )

    def finish_other(step, chunk):
        def store(head, value):
            back[step - 1, pl.ds(chunk * unit, unit), pl.ds(head * LANES, LANES)] = value

        finish(step * units + chunk, store)
        returned(step, chunk).start()

    def receive(chunks):
        begin, count = chunks[0] * unit, len(chunks) * unit
        for step in range(1, tp):
            with jax.named_scope("row_wait"):
                for chunk in chunks:
                    row_copy(step, chunk).wait_recv()
            with jax.named_scope("other_project"):
                modulate_rows(other_rows.at[step - 1], other_in, begin, count, 0, gain_scale, shift)
                project_rows(other_in, 0, count, step * units + chunks[0])

    def attend_other(chunks, phase):
        for step in range(1, tp):
            attend(step * units + chunks[0], len(chunks), phase)

    def kv_wait(step):
        with jax.named_scope("kv_wait"):
            for offset in range(1, sp):
                kv_z(step, offset).wait_recv()

    own_block.wait()
    kv_wait(0)
    with jax.named_scope("own_near"):
        attend(0, units, 0)
    for number, chunks in enumerate(plan.groups[:-1]):
        receive(chunks)
        with jax.named_scope("other_near"):
            attend_other(chunks, 0)
        if number == 0:
            weight_pair_done()
    if len(plan.groups) == 1:
        weight_pair_done()
    def weight_levels():
        for level in range(len(bits) - 1):
            with jax.named_scope("weight_dp"):
                for step in range(1, tp):
                    for copy in level_copies(step, level):
                        copy.wait_recv()
                    for copy in level_copies(step, level + 1):
                        copy.start()

    for step in range(1, tp):
        kv_wait(step)
    early = [chunk for chunks in plan.groups[:-1] for chunk in chunks]
    if early:
        with jax.named_scope("other_far"):
            attend_other(early, 1)
            for step in range(1, tp):
                for chunk in early:
                    finish_other(step, chunk)
    with jax.named_scope("own_far"):
        attend(0, units, 1)
        pl.loop(0, units)(finish_own)
    weight_levels()
    receive(plan.groups[-1])
    with jax.named_scope("other_last"):
        attend_other(plan.groups[-1], 0)
        attend_other(plan.groups[-1], 1)
        for step in range(1, tp):
            for chunk in plan.groups[-1]:
                finish_other(step, chunk)

    with jax.named_scope("weight_wait"):
        tail_load.wait()
        if bits:
            for step in range(1, tp):
                for copy in level_copies(step, len(bits) - 1):
                    copy.wait_recv()

    wide = math.gcd(plan.out_columns, 768)

    def finish_rows(start, count):
        at = pl.ds(start, count)

        def own_columns(index):
            projected[at, lanes(t * plan.out_columns + index * wide, wide)] = jnp.dot(
                branch[at, :], own_out_weight[:, lanes(index * wide, wide)],
                preferred_element_type=f32,
            ).astype(bf16)

        pl.loop(0, plan.out_columns // wide)(own_columns)
        for step in range(1, tp):
            owner = lax.rem(t + tp - step, tp)

            def other_columns(index, step=step, owner=owner):
                projected[at, lanes(owner * plan.out_columns + index * wide, wide)] = jnp.dot(
                    branch[at, :], other_out_weight[step - 1, :, lanes(index * wide, wide)],
                    preferred_element_type=f32,
                ).astype(bf16)

            pl.loop(0, plan.out_columns // wide)(other_columns)
        block = math.gcd(count, 32)
        out_gain = sums[4:5, :] * post_gain_ref[...]

        def norm_block(index):
            here = pl.ds(pl.multiple_of(start + index * block, block), block)
            values = norm_rows(projected[here, :].astype(f32))
            out_ref[here, :] = (values * out_gain).astype(bf16)

        pl.loop(0, count // block)(norm_block)

    groups = [list(range(units - 1)), [units - 1]] if units > 1 else [[0]]
    for chunks in groups:
        with jax.named_scope("back_wait"):
            for chunk in chunks:
                for step in range(1, tp):
                    returned_here(step, chunk).wait_recv()
        with jax.named_scope("tail"):
            finish_rows(chunks[0] * unit, len(chunks) * unit)

    def scatter_done(index):
        copy, valid = scatter(index)
        only(every, valid, copy.wait_send)

    each(group - 1, scatter_done)
    only(
        every, me < plan.owners,
        lambda: each(group - 1, lambda index: gather(index).wait_send()),
    )
    for step in range(1, tp):
        kv_y(step).wait_send()
        for part in range(plan.parts):
            weight_y(step, part).wait_send()
        for turn in range(1, plan.pair):
            for part in range(plan.parts):
                weight_z(step, turn, part).wait_send()
        for chunk in range(units):
            row_copy(step, chunk).wait_send()
            returned(step, chunk).wait_send()
        for level in range(len(bits)):
            for copy in level_copies(step, level):
                copy.wait_send()
    for step in range(tp):
        for offset in range(1, sp):
            kv_z(step, offset).wait_send()


def mega(plan, lambdas, small, large):
    sp, tp, dp, group = plan.sp, plan.tp, plan.dp, plan.group
    rows, model, unit, units = plan.rows, plan.model, plan.unit, plan.units
    columns, stack = plan.columns, plan.stack
    others = max(tp - 1, 1)
    turns = max(plan.pair - 1, 1)
    swaps = max(dp - 1, 1)
    bf16, f32 = jnp.bfloat16, jnp.float32
    vmem = pl.BlockSpec(memory_space=pltpu.VMEM)
    dma = pltpu.SemaphoreType.DMA
    condition = small[0].shape[1]
    return pl.pallas_call(
        functools.partial(mega_kernel, plan),
        out_shape=jax.ShapeDtypeStruct((rows, model), bf16),
        in_specs=[pl.BlockSpec(memory_space=pltpu.SMEM)]
        + [vmem] * len(small)
        + [pl.BlockSpec(memory_space=pl.ANY)] * len(large),
        out_specs=vmem,
        scratch_shapes=[
            pltpu.VMEM((3, condition, model), bf16),
            pltpu.VMEM((rows, model), bf16),
            pltpu.VMEM((plan.context, model), bf16),
            pltpu.VMEM((plan.padded, model), bf16),
            pltpu.VMEM((model, KVH * 2 * LANES), bf16),
            pltpu.VMEM((model, columns), bf16),
            pltpu.VMEM((model, columns), bf16),
            pltpu.VMEM((plan.depth, plan.out_columns), bf16),
            pltpu.VMEM((others, plan.depth, plan.out_columns), bf16),
            pltpu.VMEM((others, rows, model), bf16),
            pltpu.VMEM((len(plan.groups[0]) * unit, model), bf16),
            pltpu.VMEM((KVH, plan.padded, 2 * LANES), bf16),
            pltpu.VMEM((group * plan.padded, 3 * LANES), bf16),
            pltpu.VMEM((8, model), f32),
            pltpu.VMEM((group - 1, 8, plan.slice), f32),
            pltpu.VMEM((8, model), f32),
            pltpu.VMEM((plan.padded, model), f32),
            pltpu.VMEM((tp * units, stack, LANES), bf16),
            pltpu.VMEM((tp * units, unit, columns), bf16),
            pltpu.VMEM((plan.half, max(plan.near, plan.far)), f32),
            pltpu.VMEM((plan.half, max(plan.near, plan.far)), f32),
            pltpu.VMEM((tp * units, stack, LANES), f32),
            pltpu.VMEM((tp * units, stack, LANES), f32),
            pltpu.VMEM((tp * units, stack, LANES), f32),
            pltpu.VMEM((rows, plan.depth), bf16),
            pltpu.VMEM((others, rows, columns), bf16),
            pltpu.VMEM((rows, model), bf16),
            dma((9 + 2 * KVH,)),
            dma((group - 1,)), dma((group - 1,)), dma((group - 1,)), dma((group - 1,)),
            dma((others, units)), dma((others, units)),
            dma((others,)), dma((others,)),
            dma((tp, sp - 1)), dma((tp, sp - 1)),
            dma((others, plan.parts)), dma((others, plan.parts)),
            dma((others, turns, plan.parts)), dma((others, turns, plan.parts)),
            dma((others, plan.pair, plan.parts)), dma((others, plan.pair, plan.parts)),
            dma((others, swaps)), dma((others, swaps)),
            dma((others, units)), dma((others, units)),
        ],
        compiler_params=pltpu.CompilerParams(
            collective_id=0, has_side_effects=True, vmem_limit_bytes=63 * 2**20
        ),
    )(lambdas, *small, *large)


def local(
    sp, tp, dp,
    latents, condition, context, context_cond,
    shift_weight, scale_weight, out_gate_weight,
    pre_gain, post_gain,
    query_weight, key_weight, value_weight, head_gate_weight,
    lambdas, head_gain, out_weight,
):
    plan = Plan(
        sp, tp, dp, latents.shape[1], context.shape[1], latents.shape[2],
        out_weight.shape, query_weight.shape[1],
    )
    result = mega(
        plan,
        lambdas,
        (
            condition, context_cond[None, :], pre_gain[None, :], post_gain[None, :],
            head_gain[None, :],
        ),
        (
            latents[0], context[0], shift_weight, scale_weight, out_gate_weight,
            query_weight, key_weight, value_weight, head_gate_weight, out_weight,
        ),
    )
    return result[None]


def solution(mesh):
    return jax.shard_map(
        functools.partial(local, mesh.shape["sp"], mesh.shape["tp"], mesh.shape["dp"]),
        mesh=mesh,
        in_specs=(
            P("dp", ("sp", "tp"), None),
            P("dp", ("sp", "tp")),
            P("dp", ("sp", "tp"), None),
            P(("sp", "tp")),
            P(("sp", "tp"), None),
            P(("sp", "tp"), None),
            P(("sp", "tp"), None),
            P(),
            P(),
            P(None, "tp"),
            P(),
            P(),
            P(None, "tp"),
            P("tp"),
            P(),
            P(None, "tp"),
        ),
        out_specs=P("dp", ("sp", "tp"), None),
        check_vma=False,
    )
```

profile of v0, /device:TPU:0, one launch (start us, length us, event | category | flops | bytes accessed | tf_op | source)
XLA Modules:
  0.0 76.2 jit_solution(8926418194477059009)
XLA Ops:
  0.0 1.2 %broadcast_in_dim.15.context_cond_ref = bf16[1,384]{1,0:T(2,128)(2,1)} reshape(bf16[384]{0:T(512)(128)(2,1)} %param.19) | data formatting | bytes 1536 | tf_op jit(solution)/shard_map/broadcast_in_dim | solution.py:774
  1.2 72.3 %shard_map.154 = bf16[256,3072]{1,0:T(8,128)(2,1)} custom-call(f32[4]{0:T(128)} %lambda_ref.1, bf16[1,384]{1,0:T(2,128)(2,1)} %cond_ref.1, bf16[1,384]{1,0:T(2,128)(2,1)} %broadcast_in_dim.15.context_cond_ref, f32[1,3072]{1,0:T(1,128)} %bitcast.9, f32[1,3072]{1,0:T(1,128)} %bitcast.10, f32[1,128]{1,0:T(1,128)} %bitcast.11, bf16[256,3072]{1,0:T(8,128)(2,1)} %bitcast.7, ...), custom_call_target="tpu_custom_call" | custom-call | tf_op jit(solution)/shard_map/pallas_call | solution.py:706
  73.5 2.7 %copy.18 = bf16[1,256,3072]{2,1,0:T(8,128)(2,1)} copy(bf16[1,256,3072]{2,1,0:T(8,128)(2,1)} %bitcast.6) | data formatting | bytes 3145728
where the time goes:
time: 76.4 us; the launch traced here: 76.2 us
  Pallas kernels  72.3 us (95%)
  local copies, waits for them, and re-layouts  3.89 us (5%)
    pallas_call x1, Pallas kernels, mega(): pl.pallas_call(functools.partial(mega_kernel, plan), out_shape=jax.ShapeD...  72.3 us
    unnamed x1, local copies, waits for them, and re-layouts  2.65 us

commit v1 on v0

--- a/solution.py
+++ b/solution.py
@@ -70,7 +70,14 @@
         self.units = rows // self.unit
         self.stack = self.local_heads * 2 * self.unit
         self.half = self.stack // 2
-        self.halves = 2 if self.unit % (2 * SUBLANES) == 0 else 1
+        first = [(0, self.unit)]
+        if self.unit > SUBLANES:
+            cut = self.unit // 2 // SUBLANES * SUBLANES
+            first = [(0, cut), (cut, self.unit - cut)]
+        self.pieces = first + [(chunk * self.unit, self.unit) for chunk in range(1, self.units)]
+        self.chunk_pieces = [list(range(len(first)))] + [
+            [len(first) + chunk] for chunk in range(self.units - 1)
+        ]
         self.near = (tp + sp - 1) * self.padded
         self.far = (tp - 1) * (sp - 1) * self.padded
         self.groups = [[0]] + [[chunk] for chunk in range(1, self.units)]
@@ -205,16 +212,19 @@
             ]
         return [weight_d(step, level, index) for index in range(2**level)]
 
-    def row_copy(step, chunk):
-        at = pl.ds(chunk * unit, unit)
+    def row_copy(step, number):
+        at = pl.ds(*plan.pieces[number])
         return remote(
             latents.at[at, :], other_rows.at[step - 1, at, :],
-            row_send.at[step - 1, chunk], row_recv.at[step - 1, chunk], over_tp(step),
+            row_send.at[step - 1, number], row_recv.at[step - 1, number], over_tp(step),
         )
 
     def over_tp_steps(body):
-        for step in range(1, tp):
-            body(step)
+        if tp <= 3:
+            for step in range(1, tp):
+                body(step)
+        else:
+            pl.loop(1, tp)(body)
 
     with jax.named_scope("enter"):
         pl.semaphore_wait(barrier, group - 1 + len(bits))
@@ -232,13 +242,23 @@
                 for turn in range(1, plan.pair):
                     weight_z(step, turn, part).start()
 
+    def weight_pair(part):
+        if part < plan.parts:
+            with jax.named_scope("weight_pair"):
+                for step in range(1, tp):
+                    for turn in range(1, plan.pair):
+                        weight_z(step, turn, part).wait_recv()
+                        if bits:
+                            weight_x(step, turn, part).start()
+
     weight_start(0)
 
     with jax.named_scope("conditions"):
         conditions = []
         for ref in (cond_ref, context_cond_ref):
             value = ref[...].astype(f32)
-            conditions.append(value / (1.0 + jnp.exp(-value)))
+            value = value / (1.0 + jnp.exp(-value))
+            conditions.append(value.reshape(1, value.shape[-1]))
         depth = cond_ref.shape[1]
         index = lax.broadcasted_iota(jnp.int32, (8, depth), 0)
         first = jnp.broadcast_to(conditions[0], (8, depth))
@@ -339,7 +359,7 @@
         only(every, me < plan.owners, own_sum)
 
     weight_start(2)
-    weight_start(3)
+    over_tp_steps(lambda step: row_copy(step, 0).start())
     kv[:, 2 * LANES :] = jnp.ones((kv.shape[0], LANES), bf16)
 
     def sum_arrival(index):
@@ -348,6 +368,9 @@
 
     with jax.named_scope("gather"):
         each(group - 1, sum_arrival)
+    with jax.named_scope("weight_forward"):
+        weight_forward(0)
+        weight_forward(1)
     gain = gain_ref[...]
     shift, context_shift = sums[0:1, :], sums[1:2, :]
     gain_scale, context_gain_scale = gain * (1.0 + sums[2:3, :]), gain * (1.0 + sums[3:4, :])
@@ -400,8 +423,12 @@
     own_block = load(8 + 2 * KVH, kv_made.at[kv_group(t)], kv_slot(0, 0))
     for offset in range(1, sp):
         kv_z(0, offset).start()
-    for chunk in range(units):
-        over_tp_steps(lambda step, chunk=chunk: row_copy(step, chunk).start())
+    for number in range(1, len(plan.pieces)):
+        if number + 1 == len(plan.pieces):
+            weight_start(3)
+        over_tp_steps(lambda step, number=number: row_copy(step, number).start())
+    if len(plan.pieces) == 1:
+        weight_start(3)
 
     def project_rows(source, start, count, first_unit):
         wide = math.gcd(columns, 512)
@@ -442,25 +469,22 @@
     with jax.named_scope("kv_over_tp"):
         for step in range(1, tp):
             kv_y(step).wait_recv()
+
+    def forward():
+        for step in range(1, tp):
             for offset in range(1, sp):
                 kv_z(step, offset).start()
 
-    with jax.named_scope("weight_forward"):
-        for part in range(plan.parts):
-            weight_forward(part)
-
-    def weight_pair_done():
-        with jax.named_scope("weight_pair"):
-            for step in range(1, tp):
-                for turn in range(1, plan.pair):
-                    for part in range(plan.parts):
-                        weight_z(step, turn, part).wait_recv()
-                        if bits:
-                            weight_x(step, turn, part).start()
-
     contract = (((1,), (1,)), ((), ()))
 
-    spans = ((0, plan.near), (plan.near, plan.far))
+    here = tp * size
+    spans = {
+        "here": (0, here), "middle": (here, plan.near - here),
+        "near": (0, plan.near), "far": (plan.near, plan.far),
+    }
+
+    def follows(phase):
+        return phase in ("middle", "far")
 
     def score(buffer, index, side, phase):
         begin, count = spans[phase]
@@ -479,20 +503,21 @@
         at = pl.ds(side * plan.half, plan.half)
         scores = buffer[:, pl.ds(0, count)]
         top = jnp.max(scores, axis=-1, keepdims=True)
-        if phase:
+        if follows(phase):
             before = largest[index, at, pl.ds(0, 1)]
             top = jnp.maximum(top, before)
         both = jnp.dot(
             jnp.exp(scores - top).astype(bf16), kv[pl.ds(begin, count), pl.ds(LANES, 2 * LANES)],
             preferred_element_type=f32,
         )
-        if phase:
+        if follows(phase):
             keep = jnp.exp(before - top)
             weighted[index, at, :] = weighted[index, at, :] * keep + both[:, :LANES]
             normalizer[index, at, :] = normalizer[index, at, :] * keep + both[:, LANES:]
         else:
             weighted[index, at, :] = both[:, :LANES]
             normalizer[index, at, :] = both[:, LANES:]
+        if phase != "far":
             largest[index, at, :] = jnp.broadcast_to(top, (plan.half, LANES))
 
     def attend(first_unit, count, phase):
@@ -558,17 +583,27 @@
 
     def receive(chunks):
         begin, count = chunks[0] * unit, len(chunks) * unit
-        for step in range(1, tp):
+
+        def one(step):
             with jax.named_scope("row_wait"):
                 for chunk in chunks:
-                    row_copy(step, chunk).wait_recv()
+                    for number in plan.chunk_pieces[chunk]:
+                        row_copy(step, number).wait_recv()
             with jax.named_scope("other_project"):
                 modulate_rows(other_rows.at[step - 1], other_in, begin, count, 0, gain_scale, shift)
                 project_rows(other_in, 0, count, step * units + chunks[0])
 
+        over_tp_steps(one)
+
     def attend_other(chunks, phase):
-        for step in range(1, tp):
-            attend(step * units + chunks[0], len(chunks), phase)
+        over_tp_steps(lambda step: attend(step * units + chunks[0], len(chunks), phase))
+
+    def finish_others(chunks):
+        def one(step):
+            for chunk in chunks:
+                finish_other(step, chunk)
+
+        over_tp_steps(one)
 
     def kv_wait(step):
         with jax.named_scope("kv_wait"):
@@ -576,17 +611,23 @@
                 kv_z(step, offset).wait_recv()
 
     own_block.wait()
+    with jax.named_scope("own_here"):
+        attend(0, units, "here")
+    forward()
+    weight_forward(2)
+    weight_pair(0)
+    weight_pair(1)
     kv_wait(0)
-    with jax.named_scope("own_near"):
-        attend(0, units, 0)
+    with jax.named_scope("own_middle"):
+        attend(0, units, "middle")
     for number, chunks in enumerate(plan.groups[:-1]):
         receive(chunks)
         with jax.named_scope("other_near"):
-            attend_other(chunks, 0)
+            attend_other(chunks, "near")
         if number == 0:
-            weight_pair_done()
+            weight_pair(2)
     if len(plan.groups) == 1:
-        weight_pair_done()
+        weight_pair(2)
     def weight_levels():
         for level in range(len(bits) - 1):
             with jax.named_scope("weight_dp"):
@@ -601,34 +642,31 @@
     early = [chunk for chunks in plan.groups[:-1] for chunk in chunks]
     if early:
         with jax.named_scope("other_far"):
-            attend_other(early, 1)
-            for step in range(1, tp):
-                for chunk in early:
-                    finish_other(step, chunk)
+            attend_other(early, "far")
+            finish_others(early)
+    weight_forward(3)
     with jax.named_scope("own_far"):
-        attend(0, units, 1)
+        attend(0, units, "far")
         pl.loop(0, units)(finish_own)
-    weight_levels()
+    weight_pair(3)
     receive(plan.groups[-1])
     with jax.named_scope("other_last"):
-        attend_other(plan.groups[-1], 0)
-        attend_other(plan.groups[-1], 1)
-        for step in range(1, tp):
-            for chunk in plan.groups[-1]:
-                finish_other(step, chunk)
-
-    with jax.named_scope("weight_wait"):
-        tail_load.wait()
-        if bits:
-            for step in range(1, tp):
-                for copy in level_copies(step, len(bits) - 1):
-                    copy.wait_recv()
-
+        attend_other(plan.groups[-1], "near")
+        attend_other(plan.groups[-1], "far")
+        finish_others(plan.groups[-1])
+
+    def weights_here():
+        with jax.named_scope("weight_wait"):
+            if bits:
+                for step in range(1, tp):
+                    for copy in level_copies(step, len(bits) - 1):
+                        copy.wait_recv()
+
+    tail_load.wait()
+    weight_levels()
     wide = math.gcd(plan.out_columns, 768)
 
-    def finish_rows(start, count):
-        at = pl.ds(start, count)
-
+    def own_projection(at):
         def own_columns(index):
             projected[at, lanes(t * plan.out_columns + index * wide, wide)] = jnp.dot(
                 branch[at, :], own_out_weight[:, lanes(index * wide, wide)],
@@ -636,40 +674,59 @@
             ).astype(bf16)
 
         pl.loop(0, plan.out_columns // wide)(own_columns)
-        for step in range(1, tp):
+
+    def other_projection(at):
+        def one(step):
             owner = lax.rem(t + tp - step, tp)
 
-            def other_columns(index, step=step, owner=owner):
+            def other_columns(index):
                 projected[at, lanes(owner * plan.out_columns + index * wide, wide)] = jnp.dot(
                     branch[at, :], other_out_weight[step - 1, :, lanes(index * wide, wide)],
                     preferred_element_type=f32,
                 ).astype(bf16)
 
             pl.loop(0, plan.out_columns // wide)(other_columns)
+
+        over_tp_steps(one)
+
+    def scale_out(start, count):
         block = math.gcd(count, 32)
         out_gain = sums[4:5, :] * post_gain_ref[...]
 
-        def norm_block(index):
+        def one(index):
             here = pl.ds(pl.multiple_of(start + index * block, block), block)
             values = norm_rows(projected[here, :].astype(f32))
-            out_ref[here, :] = (values * out_gain).astype(bf16)
-
-        pl.loop(0, count // block)(norm_block)
-
+            projected[here, :] = (values * out_gain).astype(bf16)
+
+        pl.loop(0, count // block)(one)
+
+    stores = []
     groups = [list(range(units - 1)), [units - 1]] if units > 1 else [[0]]
     for chunks in groups:
         with jax.named_scope("back_wait"):
             for chunk in chunks:
                 for step in range(1, tp):
                     returned_here(step, chunk).wait_recv()
+        at = pl.ds(chunks[0] * unit, len(chunks) * unit)
         with jax.named_scope("tail"):
-            finish_rows(chunks[0] * unit, len(chunks) * unit)
+            own_projection(at)
+        if chunks is groups[0]:
+            weights_here()
+        with jax.named_scope("tail"):
+            other_projection(at)
+        with jax.named_scope("out_norm"):
+            scale_out(chunks[0] * unit, len(chunks) * unit)
+            stores.append(
+                load(9 + 2 * KVH + len(stores), projected.at[at, :], out_ref.at[at, :])
+            )
 
     def scatter_done(index):
         copy, valid = scatter(index)
         only(every, valid, copy.wait_send)
 
     each(group - 1, scatter_done)
+    for store in stores:
+        store.wait()
     only(
         every, me < plan.owners,
         lambda: each(group - 1, lambda index: gather(index).wait_send()),
@@ -681,8 +738,9 @@
         for turn in range(1, plan.pair):
             for part in range(plan.parts):
                 weight_z(step, turn, part).wait_send()
+        for number in range(len(plan.pieces)):
+            row_copy(step, number).wait_send()
         for chunk in range(units):
-            row_copy(step, chunk).wait_send()
             returned(step, chunk).wait_send()
         for level in range(len(bits)):
             for copy in level_copies(step, level):
@@ -709,7 +767,7 @@
         in_specs=[pl.BlockSpec(memory_space=pltpu.SMEM)]
         + [vmem] * len(small)
         + [pl.BlockSpec(memory_space=pl.ANY)] * len(large),
-        out_specs=vmem,
+        out_specs=pl.BlockSpec(memory_space=pl.ANY),
         scratch_shapes=[
             pltpu.VMEM((3, condition, model), bf16),
             pltpu.VMEM((rows, model), bf16),
@@ -738,9 +796,9 @@
             pltpu.VMEM((rows, plan.depth), bf16),
             pltpu.VMEM((others, rows, columns), bf16),
             pltpu.VMEM((rows, model), bf16),
-            dma((9 + 2 * KVH,)),
+            dma((11 + 2 * KVH,)),
             dma((group - 1,)), dma((group - 1,)), dma((group - 1,)), dma((group - 1,)),
-            dma((others, units)), dma((others, units)),
+            dma((others, units + 1)), dma((others, units + 1)),
             dma((others,)), dma((others,)),
             dma((tp, sp - 1)), dma((tp, sp - 1)),
             dma((others, plan.parts)), dma((others, plan.parts)),
@@ -771,7 +829,7 @@
         plan,
         lambdas,
         (
-            condition, context_cond[None, :], pre_gain[None, :], post_gain[None, :],
+            condition, context_cond, pre_gain[None, :], post_gain[None, :],
             head_gain[None, :],
         ),
         (

time: 76.4 us -> 73.4 us (0.961)
  the two profiles are of different devices: /device:TPU:0 before, /device:TPU:1 now
where the time goes in v1:
time: 73.4 us; the launch traced here: 73.3 us
  Pallas kernels  70.6 us (96%)
  local copies, waits for them, and re-layouts  2.65 us (4%)
    pallas_call x1, Pallas kernels, mega(): pl.pallas_call(functools.partial(mega_kernel, plan), out_shape=jax.ShapeD...  70.6 us
    unnamed x1, local copies, waits for them, and re-layouts  2.65 us

profile of v1, /device:TPU:1, one launch (start us, length us, event | category | flops | bytes accessed | tf_op | source)
XLA Modules:
  0.0 73.3 jit_solution(2330072530232812029)
XLA Ops:
  0.0 70.6 %shard_map.154 = bf16[256,3072]{1,0:T(8,128)(2,1)} custom-call(f32[4]{0:T(128)} %lambda_ref.1, bf16[1,384]{1,0:T(2,128)(2,1)} %cond_ref.1, bf16[384]{0:T(512)(128)(2,1)} %context_cond_ref.1, f32[1,3072]{1,0:T(1,128)} %bitcast.9, f32[1,3072]{1,0:T(1,128)} %bitcast.10, f32[1,128]{1,0:T(1,128)} %bitcast.11, bf16[256,3072]{1,0:T(8,128)(2,1)} %bitcast.7, ...), custom_call_target="tpu_custom_call" | custom-call | tf_op jit(solution)/shard_map/pallas_call | solution.py:764
  70.6 2.7 %copy.18 = bf16[1,256,3072]{2,1,0:T(8,128)(2,1)} copy(bf16[1,256,3072]{2,1,0:T(8,128)(2,1)} %bitcast.6) | data formatting | bytes 3145728
